TPU v7x, 32 devices: a whole 2x2x4 slice. The times are simulated.
32 devices in a mesh: ep: 16 (over z, x, core), tp: 2 (over y).
Axes of the slice: x: 2, y: 2, z: 4, core: 2. Of those that a mesh axis runs over, the one named last changes fastest.
Arguments:
- tokens: bfloat16 [768, 2048], P('ep', 'tp'), may hold values from -80 to 80
- pre_gain: float32 [2048], P('tp'), may hold values from 0.1 to 1.9
- post_gain: float32 [2048], P('tp'), may hold values from 0.1 to 1.9
- group_logits: float32 [768, 16], P('ep'), may hold values from -12 to 12
- expert_logits: float32 [768, 6], P('ep'), may hold values from -9 to 330
- route_group: int32 [768, 6], P('ep'), may hold values from 0 to 15, all different within a row; in each aligned block of 48 rows (0 to 47, 48 to 95, ...) at most 27 rows name the same one
- route_expert: int32 [768, 6], P('ep'), may hold values from 0 to 15
- gate_weight: bfloat16 [256, 2048, 256], P('ep', 'tp'), may hold values from -0.125 to 0.125
- up_weight: bfloat16 [256, 2048, 256], P('ep', 'tp'), may hold values from -0.125 to 0.125
- down_weight: bfloat16 [256, 256, 2048], P('ep', None, 'tp'), may hold values from -48 to 48
Outputs:
- layer_out: bfloat16 [768, 2048], P('ep', 'tp')
Inputs may be any that keep to these rules, and one draw needn't show every extreme that they name: `route_group`: each row names 6 different groups. The rows of one index of ep name any one group at most 27 times, a bound that some block reaches.
All inputs are finite; a program needn't handle non-finite values.
Results may differ from a plain program's by a relative error of at most 0.024.
Values may be sent and summed in bfloat16 or wider, within the bound.
A program may use at most 64 MiB of HBM per device.

v0:
```python
import jax
import jax.numpy as jnp
from jax import lax
from jax.sharding import PartitionSpec as P

epsilon = 1e-06


def expert_rows(rows, indices, gate_weight, up_weight, down_weight):
    experts_here = gate_weight.shape[0]
    chosen_hot = indices[None, :] == jnp.arange(experts_here, dtype=jnp.int32)[:, None]
    chosen = jnp.where(chosen_hot[:, :, None], rows[None, :, :], jnp.zeros((), jnp.bfloat16))
    part_gate = jnp.einsum(
        "esd,edf->sf", chosen, gate_weight, preferred_element_type=jnp.float32
    ).astype(jnp.bfloat16)
    part_up = jnp.einsum(
        "esd,edf->sf", chosen, up_weight, preferred_element_type=jnp.float32
    ).astype(jnp.bfloat16)
    share_gate, share_up = (
        lax.psum_scatter(part_gate, "tp", scatter_dimension=1, tiled=True).astype(jnp.float32),
        lax.psum_scatter(part_up, "tp", scatter_dimension=1, tiled=True).astype(jnp.float32),
    )
    share_hidden = (jax.nn.silu(share_gate) * share_up).astype(jnp.bfloat16)
    hidden = lax.all_gather(share_hidden, "tp", axis=1, tiled=True)
    spread = jnp.where(chosen_hot[:, :, None], hidden[None, :, :], jnp.zeros((), jnp.bfloat16))
    return jnp.einsum(
        "esf,efd->sd", spread, down_weight, preferred_element_type=jnp.float32
    ).astype(jnp.bfloat16)


def on_device(
    tokens,
    pre_gain,
    post_gain,
    group_logits,
    expert_logits,
    route_group,
    route_expert,
    gate_weight,
    up_weight,
    down_weight,
):
    tok_count, local_width = tokens.shape
    top_count = route_group.shape[1]
    group_count = lax.axis_size("ep")
    full_width = local_width * lax.axis_size("tp")
    capacity = min(
        tok_count, max(2, (3 * tok_count * top_count + 2 * group_count - 1) // (2 * group_count))
    )
    slot_count = group_count * capacity
    values = tokens.astype(jnp.float32)
    squares = lax.psum(jnp.sum(values * values, axis=1), "tp")
    normed = (values * lax.rsqrt(squares / full_width + epsilon)[:, None] * pre_gain).astype(
        jnp.bfloat16
    )
    group_table = route_group[:, :, None] == jnp.arange(group_count, dtype=jnp.int32)[None, None, :]
    picked = jnp.sum(jnp.where(group_table, group_logits[:, None, :], 0.0), axis=2)
    gates = jax.nn.softmax(picked + expert_logits, axis=-1)
    flat_group = route_group.reshape(-1)
    flat_expert = route_expert.reshape(-1)
    group_hot = (flat_group[:, None] == jnp.arange(group_count, dtype=jnp.int32)[None, :]).astype(
        jnp.int32
    )
    earlier = jnp.cumsum(group_hot, axis=0) - group_hot
    within = jnp.sum(earlier * group_hot, axis=1)
    slot_index = flat_group * capacity + within
    slot_hot = slot_index[:, None] == jnp.arange(slot_count, dtype=jnp.int32)[None, :]
    placed = slot_hot.reshape(tok_count, top_count, slot_count)
    picker = jnp.any(placed, axis=1).astype(jnp.bfloat16)
    send_rows = jnp.einsum("ts,td->sd", picker, normed, preferred_element_type=jnp.float32).astype(
        jnp.bfloat16
    )
    send_ids = jnp.sum(jnp.where(slot_hot, flat_expert[:, None] + 1, 0), axis=0) - 1
    rows = lax.all_to_all(
        send_rows.reshape(group_count, capacity, local_width),
        "ep",
        split_axis=0,
        concat_axis=0,
        tiled=True,
    )
    indices = lax.all_to_all(
        send_ids.reshape(group_count, capacity), "ep", split_axis=0, concat_axis=0, tiled=True
    )
    groups_in, items = indices.shape
    served = expert_rows(
        rows.reshape(groups_in * items, local_width),
        indices.reshape(-1),
        gate_weight,
        up_weight,
        down_weight,
    )
    answered = served.reshape(groups_in, items, local_width)
    returned = lax.all_to_all(answered, "ep", split_axis=0, concat_axis=0, tiled=True)
    weights = jnp.sum(placed.astype(jnp.float32) * gates[:, :, None], axis=1)
    mixed = jnp.dot(
        weights,
        returned.reshape(slot_count, local_width).astype(jnp.float32),
        precision=lax.Precision.HIGHEST,
    )
    totals = lax.psum(jnp.sum(mixed * mixed, axis=1), "tp")
    result = mixed * lax.rsqrt(totals / full_width + epsilon)[:, None] * post_gain
    return result.astype(jnp.bfloat16)


def solution(mesh):
    in_specs = (
        P("ep", "tp"),
        P("tp"),
        P("tp"),
        P("ep", None),
        P("ep", None),
        P("ep", None),
        P("ep", None),
        P("ep", "tp", None),
        P("ep", "tp", None),
        P("ep", None, "tp"),
    )
    out_specs = P("ep", "tp")
    return jax.shard_map(
        on_device, mesh=mesh, in_specs=in_specs, out_specs=out_specs, check_vma=False
    )
```

profile of v0, /device:TPU:0, one launch (start us, length us, event | category | flops | bytes accessed | tf_op | source)
XLA Modules:
  0.0 150.4 jit_solution(7000711114428684484)
XLA Ops:
  6.5 0.8 copy.40
  7.5 0.9 reduce-window.6
  10.5 7.4 %all-to-all-start = ((s32[16,1,27]{2,1,0:T(1,128)}), s32[16,1,27]{2,1,0:T(1,128)S(1)}, u32[]{:S(2)}, u32[]{:S(2)}) async-start(s32[16,1,27]{2,1,0:T(1,128)} %sub.21), calls=%async_computation | async-start | bytes 16384 | tf_op jit(solution)/shard_map/all_to_all | solution.py:81
  18.9 1.0 fusion.35
  19.9 4.9 %psum.14 = f32[48]{0:T(128)S(1)} all-reduce(f32[48]{0:T(128)S(1)} %fusion.35), channel_id=1, replica_groups=mesh['ep'=16,'tp'=2] {'tp'}, use_global_device_ids=true, to_apply=%region_10.11 | all-reduce | flops 48 | bytes 384 | tf_op jit(solution)/shard_map/psum | solution.py:52
  24.9 1.4 convolution_convert_fusion
  26.2 1.3 reshape.100
  27.5 6.0 %all-to-all-start.1 = ((bf16[16,27,1024]{2,1,0:T(8,128)(2,1)}), bf16[16,27,1024]{2,1,0:T(8,128)(2,1)S(1)}, u32[]{:S(2)}, u32[]{:S(2)}) async-start(bf16[16,27,1024]{2,1,0:T(8,128)(2,1)} %reshape.100), calls=%async_computation.1 | async-start | bytes 2097152 | tf_op jit(solution)/shard_map/all_to_all | solution.py:74
  34.9 21.5 %all-to-all-done.1 = bf16[16,27,1024]{2,1,0:T(8,128)(2,1)S(1)} async-done(((bf16[16,27,1024]{2,1,0:T(8,128)(2,1)}), bf16[16,27,1024]{2,1,0:T(8,128)(2,1)S(1)}, u32[]{:S(2)}, u32[]{:S(2)}) %all-to-all-start.1) | async-done | bytes 884768 | tf_op jit(solution)/shard_map/all_to_all | solution.py:74
  56.7 7.3 %fusion.26 = bf16[432,256]{1,0:T(8,128)(2,1)S(1)} fusion(bf16[16,1024,256]{2,1,0:T(8,128)(2,1)} %param.17, pred[16,432]{1,0:T(8,128)(4,1)S(1)} %iota_compare_fusion.3, bf16[432,1024]{1,0:T(8,128)(2,1)S(1)} %broadcast_in_dim.89), kind=kOutput, calls=%fused_computation.20 | convolution fusion | flops 3631067136 | bytes 9501440 | tf_op jit(solution)/shard_map/esd,edf->sf/dot_general | solution.py:13
  64.1 0.8 copy.45
  65.0 7.3 %fusion.23 = bf16[432,256]{1,0:T(8,128)(2,1)S(1)} fusion(bf16[16,1024,256]{2,1,0:T(8,128)(2,1)} %param.18, pred[16,432]{1,0:T(8,128)(4,1)S(1)} %iota_compare_fusion.3, bf16[432,1024]{1,0:T(8,128)(2,1)S(1)} %broadcast_in_dim.89), kind=kOutput, calls=%fused_computation.19 | convolution fusion | flops 3631067136 | bytes 9501440 | tf_op jit(solution)/shard_map/esd,edf->sf/dot_general | solution.py:16
  72.3 0.8 copy.47
  73.2 5.8 %reduce-scatter.7.cloned.1.call-done = bf16[128,432]{1,0:T(8,128)(2,1)} async-done(((bf16[256,432]{1,0:T(8,128)(2,1)}), bf16[128,432]{1,0:T(8,128)(2,1)}) %reduce-scatter.7.cloned.1.call-update) | async-done | bytes 110608
  79.0 1.0 copy.46
  80.1 13.0 %reduce-scatter.9.cloned.1.call-done = bf16[128,432]{1,0:T(8,128)(2,1)} async-done(((bf16[256,432]{1,0:T(8,128)(2,1)}), bf16[128,432]{1,0:T(8,128)(2,1)}) %reduce-scatter.9.cloned.1.call-update) | async-done | bytes 110608
  93.0 1.0 copy.48
  94.2 5.6 %all_gather.3 = bf16[432,256]{1,0:T(8,128)(2,1)S(1)} all-gather(bf16[432,128]{1,0:T(8,128)(2,1)S(1)} %fusion.34), channel_id=1, replica_groups=mesh['ep'=16,'tp'=2] {'tp'}, dimensions={1}, use_global_device_ids=true | all-gather | bytes 331776 | tf_op jit(solution)/shard_map/all_gather | solution.py:24
  99.8 7.3 %bitcast_convert_fusion = bf16[432,1024]{1,0:T(8,128)(2,1)S(1)} fusion(bf16[16,256,1024]{2,1,0:T(8,128)(2,1)} %param.19, pred[16,432]{1,0:T(8,128)(4,1)S(1)} %iota_compare_fusion.3, bf16[432,256]{1,0:T(8,128)(2,1)S(1)} %all_gather.3), kind=kOutput, calls=%fused_computation.13 | convolution fusion | flops 3626090496 | bytes 9501440 | tf_op jit(solution)/shard_map/esf,efd->sd/dot_general | solution.py:26
  107.1 1.3 reshape.101
  108.4 5.6 %all-to-all-start.2 = ((bf16[16,27,1024]{2,1,0:T(8,128)(2,1)}), bf16[16,27,1024]{2,1,0:T(8,128)(2,1)S(1)}, u32[]{:S(2)}, u32[]{:S(2)}) async-start(bf16[16,27,1024]{2,1,0:T(8,128)(2,1)} %reshape.101), calls=%async_computation.2 | async-start | bytes 2097152 | tf_op jit(solution)/shard_map/all_to_all | solution.py:93
  114.3 22.6 %all-to-all-done.2 = bf16[16,27,1024]{2,1,0:T(8,128)(2,1)S(1)} async-done(((bf16[16,27,1024]{2,1,0:T(8,128)(2,1)}), bf16[16,27,1024]{2,1,0:T(8,128)(2,1)S(1)}, u32[]{:S(2)}, u32[]{:S(2)}) %all-to-all-start.2) | async-done | bytes 884768 | tf_op jit(solution)/shard_map/all_to_all | solution.py:93
  137.9 4.9 %psum.15 = f32[48]{0:T(128)S(1)} all-reduce(f32[48]{0:T(128)S(1)} %get-tuple-element.7), channel_id=1, replica_groups=mesh['ep'=16,'tp'=2] {'tp'}, use_global_device_ids=true, to_apply=%region_14.15 | all-reduce | flops 48 | bytes 384 | tf_op jit(solution)/shard_map/psum | solution.py:100
  142.8 0.7 multiply_convert_fusion
  (46 shorter events, 6.3 us)
Async XLA Ops:
  10.5 17.0 %all-to-all-start = ((s32[16,1,27]{2,1,0:T(1,128)}), s32[16,1,27]{2,1,0:T(1,128)S(1)}, u32[]{:S(2)}, u32[]{:S(2)}) async-start(s32[16,1,27]{2,1,0:T(1,128)} %sub.21), calls=%async_computation | async-start | bytes 16384 | tf_op jit(solution)/shard_map/all_to_all | solution.py:81
  27.5 28.9 %all-to-all-start.1 = ((bf16[16,27,1024]{2,1,0:T(8,128)(2,1)}), bf16[16,27,1024]{2,1,0:T(8,128)(2,1)S(1)}, u32[]{:S(2)}, u32[]{:S(2)}) async-start(bf16[16,27,1024]{2,1,0:T(8,128)(2,1)} %reshape.100), calls=%async_computation.1 | async-start | bytes 2097152 | tf_op jit(solution)/shard_map/all_to_all | solution.py:74
  33.5 45.5 %reduce-scatter.7.cloned.1.call-start = ((), (), s32[]{:S(2)}) async-start(), calls=%async_computation.5 | async-start | bytes 393216
  64.9 28.1 %reduce-scatter.9.cloned.1.call-start = ((), (), s32[]{:S(2)}) async-start(), calls=%async_computation.6 | async-start | bytes 393216
  99.8 14.2 %copy-start = (s32[48,6]{0,1:T(8,128)S(1)}, s32[48,6]{0,1:T(8,128)}, u32[]{:S(2)}) copy-start(s32[48,6]{0,1:T(8,128)} %param.15) | copy-start | bytes 3460
  99.8 14.2 %copy-start.1 = (f32[48,16]{0,1:T(8,128)S(1)}, f32[48,16]{0,1:T(8,128)}, u32[]{:S(2)}) copy-start(f32[48,16]{0,1:T(8,128)} %param.13) | copy-start | bytes 9220
  99.8 14.3 %copy-start.3 = (f32[48,6]{0,1:T(8,128)S(1)}, f32[48,6]{0,1:T(8,128)}, u32[]{:S(2)}) copy-start(f32[48,6]{0,1:T(8,128)} %param.14) | copy-start | bytes 3460
  99.8 43.0 %copy-start.2 = (f32[1024]{0:T(1024)S(1)}, f32[1024]{0:T(1024)}, u32[]{:S(2)}) copy-start(f32[1024]{0:T(1024)} %param.12) | copy-start | bytes 12292
  108.4 28.5 %all-to-all-start.2 = ((bf16[16,27,1024]{2,1,0:T(8,128)(2,1)}), bf16[16,27,1024]{2,1,0:T(8,128)(2,1)S(1)}, u32[]{:S(2)}, u32[]{:S(2)}) async-start(bf16[16,27,1024]{2,1,0:T(8,128)(2,1)} %reshape.101), calls=%async_computation.2 | async-start | bytes 2097152 | tf_op jit(solution)/shard_map/all_to_all | solution.py:93
Sparse Core Ops, SparseCore 0:
  65.1 13.9 reduce-scatter.6
  81.2 11.7 reduce-scatter.8
where the time goes:
time: 152 us; the launch traced here: 150 us
  waiting for transfers between devices  63 us (41%)
  matrix products  24 us (16%)
  starting transfers between devices  19.1 us (13%)
  blocking collectives  15.5 us (10%)
  between operations  13.6 us (9%)
  local copies, waits for them, and re-layouts  9.7 us (6%)
  other arithmetic  5.49 us (4%)
    all_to_all x1, waiting for transfers between devices, on_device(): lax.all_to_all(answered, 'ep', split_axis=0, concat_axis=0, tiled=True)  22.6 us
    all_to_all x1, waiting for transfers between devices, on_device(): lax.all_to_all(send_rows.reshape(group_count, capacity, local_width), 'ep...  21.5 us
    unnamed x4, waiting for transfers between devices  18.9 us
    all_to_all x1, starting transfers between devices, on_device(): lax.all_to_all(send_ids.reshape(group_count, capacity), 'ep', split_axis=...  7.39 us
    dot_general x1, matrix products, expert_rows(): jnp.einsum('esd,edf->sf', chosen, gate_weight, preferred_element_type=jnp...  7.33 us
    dot_general x1, matrix products, expert_rows(): jnp.einsum('esd,edf->sf', chosen, up_weight, preferred_element_type=jnp.f...  7.33 us
    dot_general x1, matrix products, expert_rows(): jnp.einsum('esf,efd->sd', spread, down_weight, preferred_element_type=jnp...  7.28 us
    all_to_all x1, starting transfers between devices, on_device(): lax.all_to_all(send_rows.reshape(group_count, capacity, local_width), 'ep...  6.01 us
  transfers between devices with their start and end apart: 5, of which 4 were waited for; matrix products, arithmetic and copies ran while one was open for 10% of the time, Pallas kernels for 0%

commit v1 on v0

--- a/solution.py
+++ b/solution.py
@@ -1,9 +1,312 @@
+import functools
+
 import jax
 import jax.numpy as jnp
 from jax import lax
+from jax.experimental import pallas as pl
+from jax.experimental.pallas import tpu as pltpu
 from jax.sharding import PartitionSpec as P
 
-epsilon = 1e-06
+EPS = 1e-06
+MESH = pl.DeviceIdType.MESH
+F32 = jnp.float32
+BF16 = jnp.bfloat16
+LANES = 128
+
+
+def dot(a, b):
+    return jnp.dot(a, b, preferred_element_type=F32)
+
+
+def kernel(
+    sizes,
+    tok_ref, pre_ref, post_ref, glog_ref, elog_ref, rgrp_ref, rexp_ref,
+    gate_hbm, up_hbm, down_hbm,
+    out_ref,
+    w_for, w_own, d_own, d_for,
+    sq_mine, sq_peer, xg, xs, sel, acc, p_send, p_recv, h_own, h_for, spread, ans,
+    part, r_core, s_x, r_x, s_z, r_z, fin, t_mine, t_peer,
+    w_sem, tp_send, tp_recv, z_send, z_recv, x_send, x_recv, c_send, c_recv,
+    rc_send, rc_recv, rx_send, rx_recv, rz_send, rz_recv,
+):
+    nz, groups, cap, top, full = sizes
+    tok, width = tok_ref.shape
+    experts = gate_hbm.shape[0]
+    ff = gate_hbm.shape[2]
+    half = ff // 2
+    meta = xg.shape[3] - width
+    slots = xs.shape[0]
+    me = lax.axis_index("ep")
+    tp = lax.axis_index("tp")
+    z, x, c = me // 4, lax.rem(me // 2, 2), lax.rem(me, 2)
+    q = 2 * c + x
+    peer = {"ep": me, "tp": 1 - tp}
+    x_peer = {"ep": z * 4 + (1 - x) * 2 + c, "tp": tp}
+    c_peer = {"ep": z * 4 + x * 2 + (1 - c), "tp": tp}
+
+    def z_peer(step):
+        return {"ep": lax.rem(z + step, nz) * 4 + x * 2 + c, "tp": tp}
+
+    own_cols = pl.ds(pl.multiple_of(tp * half, half), half)
+    for_cols = pl.ds(pl.multiple_of((1 - tp) * half, half), half)
+    lo, hi = pl.ds(0, half), pl.ds(half, half)
+    loads = [
+        pltpu.make_async_copy(src, dst, w_sem.at[i])
+        for i, (src, dst) in enumerate(
+            (
+                (gate_hbm.at[:, :, for_cols], w_for.at[:, :, lo]),
+                (up_hbm.at[:, :, for_cols], w_for.at[:, :, hi]),
+                (gate_hbm.at[:, :, own_cols], w_own.at[:, :, lo]),
+                (up_hbm.at[:, :, own_cols], w_own.at[:, :, hi]),
+                (down_hbm.at[:, own_cols, :], d_own),
+                (down_hbm.at[:, for_cols, :], d_for),
+            )
+        )
+    ]
+    for load in loads:
+        load.start()
+
+    barrier = pltpu.get_barrier_semaphore()
+    for other in [peer, x_peer, c_peer] + [z_peer(s) for s in range(1, nz)]:
+        pl.semaphore_signal(barrier, inc=1, device_id=other, device_id_type=MESH)
+
+    def remote(src, dst, send, recv, target):
+        return pltpu.make_async_remote_copy(
+            src_ref=src, dst_ref=dst, send_sem=send, recv_sem=recv,
+            device_id=target, device_id_type=MESH,
+        )
+
+    values = tok_ref[...].astype(F32)
+    squares = jnp.sum(values * values, axis=1, keepdims=True)
+    sq_mine[...] = jnp.broadcast_to(squares, sq_mine.shape)
+    pl.semaphore_wait(barrier, nz + 2)
+    sq_copy = remote(sq_mine, sq_peer, tp_send.at[0], tp_recv.at[0], peer)
+    sq_copy.start()
+
+    lane = lax.broadcasted_iota(jnp.int32, (tok, meta), 1)
+    glane = lax.broadcasted_iota(jnp.int32, (tok, groups), 1)
+    logits = glog_ref[...]
+    scores, chosen = [], []
+    for k in range(top):
+        grp = rgrp_ref[:, k : k + 1]
+        chosen.append(grp)
+        picked = jnp.sum(jnp.where(glane == grp, logits, 0.0), axis=1, keepdims=True)
+        scores.append(picked + elog_ref[:, k : k + 1])
+    best = functools.reduce(jnp.maximum, scores)
+    raised = [jnp.exp(s - best) for s in scores]
+    total = functools.reduce(jnp.add, raised)
+    info = jnp.zeros((tok, meta), F32)
+    member = jnp.zeros((tok, meta), F32)
+    for k in range(top):
+        ids = rexp_ref[:, k : k + 1].astype(F32) + 1.0
+        info = info + jnp.where(lane == chosen[k], ids, 0.0)
+        info = info + jnp.where(lane == chosen[k] + 2 * groups, raised[k] / total, 0.0)
+        member = member + jnp.where(lane == chosen[k] + groups, 1.0, 0.0)
+    below = (
+        lax.broadcasted_iota(jnp.int32, (tok, tok), 0)
+        > lax.broadcasted_iota(jnp.int32, (tok, tok), 1)
+    ).astype(F32)
+    info = info + member * dot(below.astype(BF16), member.astype(BF16))
+    xg[z, q, :, width:] = info.astype(BF16)
+
+    sq_copy.wait()
+    squares = sq_mine[:, 0:1] + sq_peer[:, 0:1]
+    xg[z, q, :, :width] = (
+        values * lax.rsqrt(squares / full + EPS) * pre_ref[...]
+    ).astype(BF16)
+
+    order = sorted(range(1, nz), key=lambda s: -min(s, nz - s))
+    z_copies = {
+        s: remote(xg.at[z, q], xg.at[z, q], z_send.at[s], z_recv.at[s], z_peer(s))
+        for s in order
+    }
+    for s in order:
+        z_copies[s].start()
+    q_x = 2 * c + (1 - x)
+    x_copies, c_copies = [], []
+    for s in [0] + sorted(range(1, nz), key=lambda s: min(s, nz - s)):
+        zs = lax.rem(z + nz - s, nz)
+        if s:
+            z_copies[s].wait_recv()
+        block = xg.at[zs, q]
+        xc = remote(block, block, x_send.at[s], x_recv.at[s], x_peer)
+        xc.start()
+        cc = remote(block, block, c_send.at[s, 0], c_recv.at[s, 0], c_peer)
+        cc.start()
+        x_copies.append((s, xc))
+        c_copies.append(cc)
+    for s, xc in x_copies:
+        zs = lax.rem(z + nz - s, nz)
+        xc.wait_recv()
+        block = xg.at[zs, q_x]
+        cc = remote(block, block, c_send.at[s, 1], c_recv.at[s, 1], c_peer)
+        cc.start()
+        c_copies.append(cc)
+    for cc in c_copies:
+        cc.wait()
+    for s, xc in x_copies:
+        xc.wait_send()
+    for s in order:
+        z_copies[s].wait_send()
+
+    zt, zc = 4 * tok, 4 * cap
+
+    def slot_of(block, place):
+        return block * cap + place
+
+    def pick(i, carry):
+        rows = xg[i].reshape(zt, width + meta)
+        codes = rows[:, width:]
+        srow = lax.broadcasted_iota(jnp.int32, (16, meta), 0)
+        slane = lax.broadcasted_iota(jnp.int32, (16, meta), 1)
+        take = ((slane == me + srow * groups) & (srow < 3)).astype(F32).astype(BF16)
+        picked = lax.dot_general(
+            take, codes, (((1,), (1,)), ((), ())), preferred_element_type=F32
+        )
+        ids, place = picked[0:1, :], picked[1:2, :]
+        tcol = lax.broadcasted_iota(jnp.int32, (zc, zt), 1)
+        trow = lax.broadcasted_iota(jnp.int32, (zc, zt), 0)
+        block = functools.reduce(
+            jnp.add, [(tcol >= b * tok).astype(F32) for b in range(1, 4)]
+        )
+        hot = (trow.astype(F32) == block * cap + place) & (ids > 0.5)
+        at = pl.ds(pl.multiple_of(i * zc, 16), zc)
+        xs[at, :] = dot(hot.astype(F32).astype(BF16), rows[:, :width]).astype(BF16)
+        sel[at, :] = jnp.broadcast_to(
+            jnp.sum(jnp.where(hot, ids, 0.0), axis=1, keepdims=True), (zc, LANES)
+        )
+        return carry
+
+    lax.fori_loop(0, nz, pick, 0)
+
+    def project(weights):
+        acc[...] = jnp.zeros_like(acc)
+
+        def step(e, carry):
+            on = (sel[...] == (e + 1).astype(F32)).astype(F32).astype(BF16)
+            on = jnp.concatenate([on] * (width // LANES), axis=1)
+            acc[...] += dot(xs[...] * on, weights[e])
+            return carry
+
+        lax.fori_loop(0, experts, step, 0)
+
+    loads[0].wait()
+    loads[1].wait()
+    project(w_for)
+    p_send[...] = acc[...].astype(BF16)
+    p_copy = remote(p_send, p_recv, tp_send.at[1], tp_recv.at[1], peer)
+    p_copy.start()
+    loads[2].wait()
+    loads[3].wait()
+    project(w_own)
+    p_copy.wait()
+    pre = acc[...].astype(BF16).astype(F32) + p_recv[...].astype(F32)
+    g, u = pre[:, :half], pre[:, half:]
+    h_own[...] = (g / (1.0 + jnp.exp(-g)) * u).astype(BF16)
+    h_copy = remote(h_own, h_for, tp_send.at[2], tp_recv.at[2], peer)
+    h_copy.start()
+
+    tile = 256 if width % 256 == 0 else LANES
+
+    def down(hidden, weights, first):
+        for e in range(experts):
+            on = (sel[...] == float(e + 1)).astype(F32).astype(BF16)
+            if half != LANES:
+                on = jnp.concatenate([on] * (half // LANES), axis=1)
+            spread[:, e * half : (e + 1) * half] = hidden[...] * on
+
+        def step(j, carry):
+            at = pl.ds(pl.multiple_of(j * tile, tile), tile)
+            w = weights[:, :, at].reshape(experts * half, tile)
+            got = dot(spread[...], w)
+            ans[:, at] = got if first else ans[:, at] + got
+            return carry
+
+        lax.fori_loop(0, width // tile, step, 0)
+
+    loads[4].wait()
+    down(h_own, d_own, True)
+    loads[5].wait()
+    h_copy.wait()
+    down(h_for, d_for, False)
+
+    def combine(i, carry):
+        codes = xg[i, :, :, width:].reshape(zt, meta).astype(F32)
+        clane = lax.broadcasted_iota(jnp.int32, (zt, meta), 1)
+
+        def column(j):
+            return jnp.sum(
+                jnp.where(clane == me + j * groups, codes, 0.0), axis=1, keepdims=True
+            )
+
+        ids, place, gate = column(0), column(1), column(2)
+        trow = lax.broadcasted_iota(jnp.int32, (zt, zc), 0)
+        tcol = lax.broadcasted_iota(jnp.int32, (zt, zc), 1).astype(F32)
+        block = functools.reduce(
+            jnp.add, [(trow >= b * tok).astype(F32) for b in range(1, 4)]
+        )
+        hot = (tcol == block * cap + place) & (ids > 0.5)
+        mix = jnp.where(hot, gate, 0.0).astype(BF16)
+        at = pl.ds(pl.multiple_of(i * zc, 16), zc)
+        got = dot(mix, ans[at, :].astype(BF16))
+        part[i] = got.astype(BF16).reshape(4, tok, width)
+        return carry
+
+    lax.fori_loop(0, nz, combine, 0)
+
+    far = order + [0]
+    core_copies = {}
+    for s in far:
+        zs = lax.rem(z + s, nz)
+        core_copies[s] = remote(
+            part.at[zs, pl.ds(2 * (1 - c), 2)], r_core.at[zs],
+            rc_send.at[s], rc_recv.at[s], c_peer,
+        )
+        core_copies[s].start()
+    rx_copies = {}
+    for s in far:
+        zs = lax.rem(z + s, nz)
+        core_copies[s].wait_recv()
+        s_x[zs] = (
+            part[zs, 2 * c + (1 - x)].astype(F32) + r_core[zs, 1 - x].astype(F32)
+        ).astype(BF16)
+        rx_copies[s] = remote(s_x.at[zs], r_x.at[zs], rx_send.at[s], rx_recv.at[s], x_peer)
+        rx_copies[s].start()
+    rz_copies = {}
+    for s in far:
+        zs = lax.rem(z + s, nz)
+        rx_copies[s].wait_recv()
+        summed = (
+            part[zs, q].astype(F32) + r_core[zs, x].astype(F32) + r_x[zs].astype(F32)
+        )
+        if s:
+            s_z[s] = summed.astype(BF16)
+            rz_copies[s] = remote(
+                s_z.at[s], r_z.at[s], rz_send.at[s], rz_recv.at[s], z_peer(s)
+            )
+            rz_copies[s].start()
+        else:
+            fin[...] = summed
+    mixed = fin[...]
+    for s in order:
+        rz_copies[s].wait_recv()
+        mixed = mixed + r_z[s].astype(F32)
+    fin[...] = mixed
+    t_mine[...] = jnp.broadcast_to(
+        jnp.sum(mixed * mixed, axis=1, keepdims=True), t_mine.shape
+    )
+    t_copy = remote(t_mine, t_peer, tp_send.at[3], tp_recv.at[3], peer)
+    t_copy.start()
+    for s in far:
+        core_copies[s].wait_send()
+        rx_copies[s].wait_send()
+        if s:
+            rz_copies[s].wait_send()
+    t_copy.wait()
+    totals = t_mine[:, 0:1] + t_peer[:, 0:1]
+    out_ref[...] = (
+        fin[...] * lax.rsqrt(totals / full + EPS) * post_ref[...]
+    ).astype(BF16)
 
 
 def expert_rows(rows, indices, gate_weight, up_weight, down_weight):
@@ -28,7 +331,7 @@
     ).astype(jnp.bfloat16)
 
 
-def on_device(
+def any_mesh(
     tokens,
     pre_gain,
     post_gain,
@@ -50,7 +353,7 @@
     slot_count = group_count * capacity
     values = tokens.astype(jnp.float32)
     squares = lax.psum(jnp.sum(values * values, axis=1), "tp")
-    normed = (values * lax.rsqrt(squares / full_width + epsilon)[:, None] * pre_gain).astype(
+    normed = (values * lax.rsqrt(squares / full_width + EPS)[:, None] * pre_gain).astype(
         jnp.bfloat16
     )
     group_table = route_group[:, :, None] == jnp.arange(group_count, dtype=jnp.int32)[None, None, :]
@@ -98,24 +401,83 @@
         precision=lax.Precision.HIGHEST,
     )
     totals = lax.psum(jnp.sum(mixed * mixed, axis=1), "tp")
-    result = mixed * lax.rsqrt(totals / full_width + epsilon)[:, None] * post_gain
+    result = mixed * lax.rsqrt(totals / full_width + EPS)[:, None] * post_gain
     return result.astype(jnp.bfloat16)
+
+
+def on_device(
+    tokens, pre_gain, post_gain, group_logits, expert_logits, route_group, route_expert,
+    gate_weight, up_weight, down_weight,
+):
+    tok, width = tokens.shape
+    top = route_group.shape[1]
+    groups = lax.axis_size("ep")
+    if lax.axis_size("tp") != 2 or groups % 4 or width % LANES or gate_weight.shape[2] % 256:
+        return any_mesh(
+            tokens, pre_gain, post_gain, group_logits, expert_logits, route_group,
+            route_expert, gate_weight, up_weight, down_weight,
+        )
+    nz = groups // 4
+    full = width * lax.axis_size("tp")
+    cap = min(tok, max(2, (3 * tok * top + 2 * groups - 1) // (2 * groups)))
+    cap = (4 * cap + 15) // 16 * 4
+    slots = groups * cap
+    experts, _, ff = gate_weight.shape
+    half = ff // 2
+    meta = (3 * groups + LANES - 1) // LANES * LANES
+    vmem = pl.BlockSpec(memory_space=pltpu.VMEM)
+    hbm = pl.BlockSpec(memory_space=pl.ANY)
+    dma = pltpu.SemaphoreType.DMA
+    scratch = [
+        pltpu.VMEM((experts, width, ff), BF16),
+        pltpu.VMEM((experts, width, ff), BF16),
+        pltpu.VMEM((experts, half, width), BF16),
+        pltpu.VMEM((experts, half, width), BF16),
+        pltpu.VMEM((tok, LANES), F32),
+        pltpu.VMEM((tok, LANES), F32),
+        pltpu.VMEM((nz, 4, tok, width + meta), BF16),
+        pltpu.VMEM((slots, width), BF16),
+        pltpu.VMEM((slots, LANES), F32),
+        pltpu.VMEM((slots, ff), F32),
+        pltpu.VMEM((slots, ff), BF16),
+        pltpu.VMEM((slots, ff), BF16),
+        pltpu.VMEM((slots, half), BF16),
+        pltpu.VMEM((slots, half), BF16),
+        pltpu.VMEM((slots, experts * half), BF16),
+        pltpu.VMEM((slots, width), F32),
+        pltpu.VMEM((nz, 4, tok, width), BF16),
+        pltpu.VMEM((nz, 2, tok, width), BF16),
+        pltpu.VMEM((nz, tok, width), BF16),
+        pltpu.VMEM((nz, tok, width), BF16),
+        pltpu.VMEM((nz, tok, width), BF16),
+        pltpu.VMEM((nz, tok, width), BF16),
+        pltpu.VMEM((tok, width), F32),
+        pltpu.VMEM((tok, LANES), F32),
+        pltpu.VMEM((tok, LANES), F32),
+        dma((6,)), dma((4,)), dma((4,)),
+        dma((nz,)), dma((nz,)), dma((nz,)), dma((nz,)), dma((nz, 2)), dma((nz, 2)),
+        dma((nz,)), dma((nz,)), dma((nz,)), dma((nz,)), dma((nz,)), dma((nz,)),
+    ]
+    return pl.pallas_call(
+        functools.partial(kernel, (nz, groups, cap, top, full)),
+        out_shape=jax.ShapeDtypeStruct((tok, width), BF16),
+        in_specs=[vmem] * 7 + [hbm] * 3,
+        out_specs=vmem,
+        scratch_shapes=scratch,
+        compiler_params=pltpu.CompilerParams(
+            collective_id=0, has_side_effects=True, vmem_limit_bytes=63 * 1024 * 1024
+        ),
+    )(
+        tokens, pre_gain.reshape(1, width), post_gain.reshape(1, width), group_logits,
+        expert_logits, route_group, route_expert, gate_weight, up_weight, down_weight,
+    )
 
 
 def solution(mesh):
     in_specs = (
-        P("ep", "tp"),
-        P("tp"),
-        P("tp"),
-        P("ep", None),
-        P("ep", None),
-        P("ep", None),
-        P("ep", None),
-        P("ep", "tp", None),
-        P("ep", "tp", None),
-        P("ep", None, "tp"),
-    )
-    out_specs = P("ep", "tp")
+        P("ep", "tp"), P("tp"), P("tp"), P("ep", None), P("ep", None), P("ep", None),
+        P("ep", None), P("ep", "tp", None), P("ep", "tp", None), P("ep", None, "tp"),
+    )
     return jax.shard_map(
-        on_device, mesh=mesh, in_specs=in_specs, out_specs=out_specs, check_vma=False
-    )
+        on_device, mesh=mesh, in_specs=in_specs, out_specs=P("ep", "tp"), check_vma=False
+    )

time: 152 us -> 76.7 us (0.50)
  Pallas kernels: 0 us -> 69.4 us
  waiting for transfers between devices: 63 us -> 0 us
  matrix products: 24 us -> 0 us
  starting transfers between devices: 19.1 us -> 0 us
  blocking collectives: 15.5 us -> 0 us
  between operations: 13.6 us -> 0.01 us
  other arithmetic: 5.49 us -> 0 us
  local copies, waits for them, and re-layouts: 9.7 us -> 7.03 us
    pallas_call x0 -> x1, Pallas kernels: none -> 69.4 us  [on_device(): pl.pallas_call(functools.partial(kernel, (nz, groups, cap, top, full)), o...]
    all_to_all x3 -> x0, waiting for transfers between devices: 44.2 us -> none  [the longest x1 22.6 us: on_device(): lax.all_to_all(answered, 'ep', split_axis=0, concat_axis=0, tiled=True)]
    dot_general x5 -> x0, matrix products: 24 us -> none  [the longest x1 7.33 us: expert_rows(): jnp.einsum('esd,edf->sf', chosen, gate_weight, preferred_element_type=jnp...]
    all_to_all x3 -> x0, starting transfers between devices: 19 us -> none  [the longest x1 7.39 us: on_device(): lax.all_to_all(send_ids.reshape(group_count, capacity), 'ep', split_axis=...]
    unnamed x4 -> x0, waiting for transfers between devices: 18.9 us -> none
    psum x2 -> x0, blocking collectives: 9.86 us -> none  [the longest x1 4.93 us: on_device(): squares = lax.psum(jnp.sum(values * values, axis=1), 'tp')]
    all_gather x1 -> x0, blocking collectives: 5.63 us -> none  [expert_rows(): hidden = lax.all_gather(share_hidden, 'tp', axis=1, tiled=True)]
    reshape x3 -> x0, local copies, waits for them, and re-layouts: 2.84 us -> none  [the longest x1 1.28 us: on_device(): send_rows.reshape(group_count, capacity, local_width)]
  transfers between devices with their start and end apart: 5 -> 0, of which waited for: 4 -> 0; matrix products, arithmetic and copies ran while one was open for 10% -> 0% of each run, Pallas kernels for 0% -> 0%
where the time goes in v1:
time: 76.7 us; the launch traced here: 76.4 us
  Pallas kernels  69.4 us (90%)
  local copies, waits for them, and re-layouts  7.03 us (9%)
    pallas_call x1, Pallas kernels, on_device(): pl.pallas_call(functools.partial(kernel, (nz, groups, cap, top, full)), o...  69.4 us
    unnamed x5, local copies, waits for them, and re-layouts  7.03 us

profile of v1, /device:TPU:0, one launch (start us, length us, event | category | flops | bytes accessed | tf_op | source)
XLA Modules:
  0.0 76.4 jit_solution(13921164768299110728)
XLA Ops:
  0.0 1.4 %copy.11.glog_ref = f32[48,16]{1,0:T(8,128)} copy(f32[48,16]{0,1:T(8,128)} %param.13) | data formatting | bytes 6144 | tf_op args[3]
  1.4 1.4 %copy.12.elog_ref = f32[48,6]{1,0:T(8,128)} copy(f32[48,6]{0,1:T(8,128)} %param.14) | data formatting | bytes 2304 | tf_op args[4]
  2.8 1.4 %copy.13.rgrp_ref = s32[48,6]{1,0:T(8,128)} copy(s32[48,6]{0,1:T(8,128)} %param.15) | data formatting | bytes 2304 | tf_op args[5]
  4.1 1.4 %copy.14.rexp_ref = s32[48,6]{1,0:T(8,128)} copy(s32[48,6]{0,1:T(8,128)} %param.16) | data formatting | bytes 2304 | tf_op args[6]
  5.5 69.4 %shard_map.100 = bf16[48,1024]{1,0:T(8,128)(2,1)} custom-call(bf16[48,1024]{1,0:T(8,128)(2,1)} %tok_ref.1, f32[1,1024]{1,0:T(1,128)} %bitcast.2, f32[1,1024]{1,0:T(1,128)} %bitcast.3, f32[48,16]{1,0:T(8,128)} %copy.11.glog_ref, f32[48,6]{1,0:T(8,128)} %copy.12.elog_ref, s32[48,6]{1,0:T(8,128)} %copy.13.rgrp_ref, s32[48,6]{1,0:T(8,128)} %copy.14.rexp_ref, ...), custom_call_target="tpu_custom_call" | custom-call | tf_op jit(solution)/shard_map/pallas_call | solution.py:461
  74.9 1.5 %copy.16 = bf16[48,1024]{1,0:T(8,128)(2,1)} copy(bf16[48,1024]{1,0:T(8,128)(2,1)} %shard_map.100) | data formatting | bytes 196608

commit v2 on v1

--- a/solution.py
+++ b/solution.py
@@ -24,7 +24,7 @@
     gate_hbm, up_hbm, down_hbm,
     out_ref,
     w_for, w_own, d_own, d_for,
-    sq_mine, sq_peer, xg, xs, sel, acc, p_send, p_recv, h_own, h_for, spread, ans,
+    sq_mine, sq_peer, xg, xs, sel, own, p_send, p_recv, h_own, h_for, spread, ans,
     part, r_core, s_x, r_x, s_z, r_z, fin, t_mine, t_peer,
     w_sem, tp_send, tp_recv, z_send, z_recv, x_send, x_recv, c_send, c_recv,
     rc_send, rc_recv, rx_send, rx_recv, rz_send, rz_recv,
@@ -123,38 +123,31 @@
     for s in order:
         z_copies[s].start()
     q_x = 2 * c + (1 - x)
-    x_copies, c_copies = [], []
-    for s in [0] + sorted(range(1, nz), key=lambda s: min(s, nz - s)):
-        zs = lax.rem(z + nz - s, nz)
+    near = [0] + order[::-1]
+    x_copies, c_copies = {}, {}
+
+    def forward_own(s):
         if s:
             z_copies[s].wait_recv()
-        block = xg.at[zs, q]
-        xc = remote(block, block, x_send.at[s], x_recv.at[s], x_peer)
-        xc.start()
+        block = xg.at[lax.rem(z + nz - s, nz), q]
+        x_copies[s] = remote(block, block, x_send.at[s], x_recv.at[s], x_peer)
+        x_copies[s].start()
         cc = remote(block, block, c_send.at[s, 0], c_recv.at[s, 0], c_peer)
         cc.start()
-        x_copies.append((s, xc))
-        c_copies.append(cc)
-    for s, xc in x_copies:
-        zs = lax.rem(z + nz - s, nz)
-        xc.wait_recv()
-        block = xg.at[zs, q_x]
+        c_copies[s] = [cc]
+
+    def forward_side(s):
+        x_copies[s].wait_recv()
+        block = xg.at[lax.rem(z + nz - s, nz), q_x]
         cc = remote(block, block, c_send.at[s, 1], c_recv.at[s, 1], c_peer)
         cc.start()
-        c_copies.append(cc)
-    for cc in c_copies:
-        cc.wait()
-    for s, xc in x_copies:
-        xc.wait_send()
-    for s in order:
-        z_copies[s].wait_send()
+        c_copies[s].append(cc)
+        for copy in c_copies[s]:
+            copy.wait_recv()
 
     zt, zc = 4 * tok, 4 * cap
 
-    def slot_of(block, place):
-        return block * cap + place
-
-    def pick(i, carry):
+    def pick(i):
         rows = xg[i].reshape(zt, width + meta)
         codes = rows[:, width:]
         srow = lax.broadcasted_iota(jnp.int32, (16, meta), 0)
@@ -175,62 +168,78 @@
         sel[at, :] = jnp.broadcast_to(
             jnp.sum(jnp.where(hot, ids, 0.0), axis=1, keepdims=True), (zc, LANES)
         )
-        return carry
-
-    lax.fori_loop(0, nz, pick, 0)
-
-    def project(weights):
-        acc[...] = jnp.zeros_like(acc)
-
-        def step(e, carry):
-            on = (sel[...] == (e + 1).astype(F32)).astype(F32).astype(BF16)
+
+    def project(at, weights):
+        def step(e, total):
+            on = (sel[at, :] == (e + 1).astype(F32)).astype(F32).astype(BF16)
             on = jnp.concatenate([on] * (width // LANES), axis=1)
-            acc[...] += dot(xs[...] * on, weights[e])
-            return carry
-
-        lax.fori_loop(0, experts, step, 0)
-
-    loads[0].wait()
-    loads[1].wait()
-    project(w_for)
-    p_send[...] = acc[...].astype(BF16)
-    p_copy = remote(p_send, p_recv, tp_send.at[1], tp_recv.at[1], peer)
-    p_copy.start()
-    loads[2].wait()
-    loads[3].wait()
-    project(w_own)
-    p_copy.wait()
-    pre = acc[...].astype(BF16).astype(F32) + p_recv[...].astype(F32)
-    g, u = pre[:, :half], pre[:, half:]
-    h_own[...] = (g / (1.0 + jnp.exp(-g)) * u).astype(BF16)
-    h_copy = remote(h_own, h_for, tp_send.at[2], tp_recv.at[2], peer)
-    h_copy.start()
+            return total + dot(xs[at, :] * on, weights[e])
+
+        return lax.fori_loop(0, experts, step, jnp.zeros((zc, ff), F32))
+
+    p_copies, h_copies = {}, {}
+
+    def rows_of(s):
+        return pl.ds(pl.multiple_of(lax.rem(z + nz - s, nz) * zc, 16), zc)
+
+    def finish(s):
+        at = rows_of(s)
+        p_copies[s].wait_recv()
+        pre = own[at, :].astype(F32) + p_recv[at, :].astype(F32)
+        g, u = pre[:, :half], pre[:, half:]
+        h_own[at, :] = (g / (1.0 + jnp.exp(-g)) * u).astype(BF16)
+        h_copies[s] = remote(
+            h_own.at[at], h_for.at[at], tp_send.at[2 + nz + s], tp_recv.at[2 + nz + s], peer
+        )
+        h_copies[s].start()
+
+    forward_own(near[0])
+    for n, s in enumerate(near):
+        if n + 1 < nz:
+            forward_own(near[n + 1])
+        forward_side(s)
+        pick(lax.rem(z + nz - s, nz))
+        at = rows_of(s)
+        if n == 0:
+            for load in loads[:4]:
+                load.wait()
+        p_send[at, :] = project(at, w_for).astype(BF16)
+        p_copies[s] = remote(
+            p_send.at[at], p_recv.at[at], tp_send.at[2 + s], tp_recv.at[2 + s], peer
+        )
+        p_copies[s].start()
+        own[at, :] = project(at, w_own).astype(BF16)
+        if n:
+            finish(near[n - 1])
+    finish(near[-1])
+    for s in near:
+        x_copies[s].wait_send()
+        for copy in c_copies[s]:
+            copy.wait_send()
+        if s:
+            z_copies[s].wait_send()
 
     tile = 256 if width % 256 == 0 else LANES
 
-    def down(hidden, weights, first):
+    def down(at):
         for e in range(experts):
-            on = (sel[...] == float(e + 1)).astype(F32).astype(BF16)
+            on = (sel[at, :] == float(e + 1)).astype(F32).astype(BF16)
             if half != LANES:
                 on = jnp.concatenate([on] * (half // LANES), axis=1)
-            spread[:, e * half : (e + 1) * half] = hidden[...] * on
+            cols = slice(e * half, (e + 1) * half)
+            spread[0, :, cols] = h_own[at, :] * on
+            spread[1, :, cols] = h_for[at, :] * on
 
         def step(j, carry):
-            at = pl.ds(pl.multiple_of(j * tile, tile), tile)
-            w = weights[:, :, at].reshape(experts * half, tile)
-            got = dot(spread[...], w)
-            ans[:, at] = got if first else ans[:, at] + got
+            cols = pl.ds(pl.multiple_of(j * tile, tile), tile)
+            one = dot(spread[0], d_own[:, :, cols].reshape(experts * half, tile))
+            two = dot(spread[1], d_for[:, :, cols].reshape(experts * half, tile))
+            ans[:, cols] = (one + two).astype(BF16)
             return carry
 
         lax.fori_loop(0, width // tile, step, 0)
 
-    loads[4].wait()
-    down(h_own, d_own, True)
-    loads[5].wait()
-    h_copy.wait()
-    down(h_for, d_for, False)
-
-    def combine(i, carry):
+    def combine(i):
         codes = xg[i, :, :, width:].reshape(zt, meta).astype(F32)
         clane = lax.broadcasted_iota(jnp.int32, (zt, meta), 1)
 
@@ -247,24 +256,13 @@
         )
         hot = (tcol == block * cap + place) & (ids > 0.5)
         mix = jnp.where(hot, gate, 0.0).astype(BF16)
-        at = pl.ds(pl.multiple_of(i * zc, 16), zc)
-        got = dot(mix, ans[at, :].astype(BF16))
-        part[i] = got.astype(BF16).reshape(4, tok, width)
-        return carry
-
-    lax.fori_loop(0, nz, combine, 0)
-
-    far = order + [0]
-    core_copies = {}
-    for s in far:
-        zs = lax.rem(z + s, nz)
-        core_copies[s] = remote(
-            part.at[zs, pl.ds(2 * (1 - c), 2)], r_core.at[zs],
-            rc_send.at[s], rc_recv.at[s], c_peer,
-        )
-        core_copies[s].start()
-    rx_copies = {}
-    for s in far:
+        part[i] = dot(mix, ans[...]).astype(BF16).reshape(4, tok, width)
+
+    loads[4].wait()
+    loads[5].wait()
+    core_copies, rx_copies = {}, {}
+
+    def send_side(s):
         zs = lax.rem(z + s, nz)
         core_copies[s].wait_recv()
         s_x[zs] = (
@@ -272,6 +270,23 @@
         ).astype(BF16)
         rx_copies[s] = remote(s_x.at[zs], r_x.at[zs], rx_send.at[s], rx_recv.at[s], x_peer)
         rx_copies[s].start()
+
+    back = near[1:] + [0]
+    for s in back:
+        zs = lax.rem(z + nz - s, nz)
+        h_copies[s].wait_recv()
+        down(rows_of(s))
+        combine(zs)
+        core_copies[nz - s if s else 0] = copy = remote(
+            part.at[zs, pl.ds(2 * (1 - c), 2)], r_core.at[zs],
+            rc_send.at[s], rc_recv.at[s], c_peer,
+        )
+        copy.start()
+        if s != back[0]:
+            send_side(last)
+        last = nz - s if s else 0
+    send_side(last)
+    far = list(rx_copies)
     rz_copies = {}
     for s in far:
         zs = lax.rem(z + s, nz)
@@ -295,8 +310,11 @@
     t_mine[...] = jnp.broadcast_to(
         jnp.sum(mixed * mixed, axis=1, keepdims=True), t_mine.shape
     )
-    t_copy = remote(t_mine, t_peer, tp_send.at[3], tp_recv.at[3], peer)
+    t_copy = remote(t_mine, t_peer, tp_send.at[1], tp_recv.at[1], peer)
     t_copy.start()
+    for s in near:
+        p_copies[s].wait_send()
+        h_copies[s].wait_send()
     for s in far:
         core_copies[s].wait_send()
         rx_copies[s].wait_send()
@@ -438,13 +456,13 @@
         pltpu.VMEM((nz, 4, tok, width + meta), BF16),
         pltpu.VMEM((slots, width), BF16),
         pltpu.VMEM((slots, LANES), F32),
-        pltpu.VMEM((slots, ff), F32),
+        pltpu.VMEM((slots, ff), BF16),
         pltpu.VMEM((slots, ff), BF16),
         pltpu.VMEM((slots, ff), BF16),
         pltpu.VMEM((slots, half), BF16),
         pltpu.VMEM((slots, half), BF16),
-        pltpu.VMEM((slots, experts * half), BF16),
-        pltpu.VMEM((slots, width), F32),
+        pltpu.VMEM((2, 4 * cap, experts * half), BF16),
+        pltpu.VMEM((4 * cap, width), BF16),
         pltpu.VMEM((nz, 4, tok, width), BF16),
         pltpu.VMEM((nz, 2, tok, width), BF16),
         pltpu.VMEM((nz, tok, width), BF16),
@@ -454,7 +472,7 @@
         pltpu.VMEM((tok, width), F32),
         pltpu.VMEM((tok, LANES), F32),
         pltpu.VMEM((tok, LANES), F32),
-        dma((6,)), dma((4,)), dma((4,)),
+        dma((6,)), dma((2 * nz + 2,)), dma((2 * nz + 2,)),
         dma((nz,)), dma((nz,)), dma((nz,)), dma((nz,)), dma((nz, 2)), dma((nz, 2)),
         dma((nz,)), dma((nz,)), dma((nz,)), dma((nz,)), dma((nz,)), dma((nz,)),
     ]

time: 76.7 us -> 88.1 us (1.15)
  Pallas kernels: 69.4 us -> 80.7 us
    pallas_call x1, Pallas kernels: 69.4 us -> 80.7 us  [on_device(): pl.pallas_call(functools.partial(kernel, (nz, groups, cap, top, full)), o...]
where the time goes in v2:
time: 88.1 us; the launch traced here: 87.8 us
  Pallas kernels  80.7 us (92%)
  local copies, waits for them, and re-layouts  7.03 us (8%)
    pallas_call x1, Pallas kernels, on_device(): pl.pallas_call(functools.partial(kernel, (nz, groups, cap, top, full)), o...  80.7 us
    unnamed x5, local copies, waits for them, and re-layouts  7.03 us

profile of v2, /device:TPU:0, one launch (start us, length us, event | category | flops | bytes accessed | tf_op | source)
XLA Modules:
  0.0 87.8 jit_solution(18116051370104131289)
XLA Ops:
  0.0 1.4 %copy.11.glog_ref = f32[48,16]{1,0:T(8,128)} copy(f32[48,16]{0,1:T(8,128)} %param.13) | data formatting | bytes 6144 | tf_op args[3]
  1.4 1.4 %copy.12.elog_ref = f32[48,6]{1,0:T(8,128)} copy(f32[48,6]{0,1:T(8,128)} %param.14) | data formatting | bytes 2304 | tf_op args[4]
  2.8 1.4 %copy.13.rgrp_ref = s32[48,6]{1,0:T(8,128)} copy(s32[48,6]{0,1:T(8,128)} %param.15) | data formatting | bytes 2304 | tf_op args[5]
  4.1 1.4 %copy.14.rexp_ref = s32[48,6]{1,0:T(8,128)} copy(s32[48,6]{0,1:T(8,128)} %param.16) | data formatting | bytes 2304 | tf_op args[6]
  5.5 80.7 %shard_map.100 = bf16[48,1024]{1,0:T(8,128)(2,1)} custom-call(bf16[48,1024]{1,0:T(8,128)(2,1)} %tok_ref.1, f32[1,1024]{1,0:T(1,128)} %bitcast.2, f32[1,1024]{1,0:T(1,128)} %bitcast.3, f32[48,16]{1,0:T(8,128)} %copy.11.glog_ref, f32[48,6]{1,0:T(8,128)} %copy.12.elog_ref, s32[48,6]{1,0:T(8,128)} %copy.13.rgrp_ref, s32[48,6]{1,0:T(8,128)} %copy.14.rexp_ref, ...), custom_call_target="tpu_custom_call" | custom-call | tf_op jit(solution)/shard_map/pallas_call | solution.py:479
  86.2 1.5 %copy.16 = bf16[48,1024]{1,0:T(8,128)(2,1)} copy(bf16[48,1024]{1,0:T(8,128)(2,1)} %shard_map.100) | data formatting | bytes 196608
